TPU v7x, 32 devices: a whole 2x2x4 slice. The times are simulated.
32 devices in a mesh: ep: 8 (over z, y), tp: 4 (over x, core).
Axes of the slice: x: 2, y: 2, z: 4, core: 2. Of those that a mesh axis runs over, the one named last changes fastest.
Arguments:
- tokens: bfloat16 [2048, 2048], P('ep'), may hold values from -6 to 6
- cotangent: bfloat16 [2048, 2048], P('ep'), may hold values from -6 to 6
- gate_weights: bfloat16 [2048, 2], P('ep'), may hold values from 0.099609375 to 0.8984375
- routes: int32 [2048, 2], P('ep'), may hold values from 0 to 7, all different within a row; in each aligned block of 256 rows (0 to 255, 256 to 511, ...) at most 96 rows name the same one
- w_gate: bfloat16 [8, 2048, 3584], P('ep', None, 'tp'), may hold values from -0.125 to 0.125
- w_up: bfloat16 [8, 2048, 3584], P('ep', None, 'tp'), may hold values from -0.125 to 0.125
- w_down: bfloat16 [8, 3584, 2048], P('ep', 'tp'), may hold values from -0.09375 to 0.09375
Outputs:
- grad_tokens: bfloat16 [2048, 2048], P('ep', 'tp')
- grad_gates: float32 [2048, 2], P('ep')
- grad_w_gate: bfloat16 [8, 2048, 3584], P('ep', None, 'tp')
- grad_w_up: bfloat16 [8, 2048, 3584], P('ep', None, 'tp')
- grad_w_down: bfloat16 [8, 3584, 2048], P('ep', 'tp')
Inputs may be any that keep to these rules, and one draw needn't show every extreme that they name: `routes`: each row names 2 different experts. Among the rows of one index of ep no expert is named by more than 96 rows, and this bound is reached in every draw.
All inputs are finite; a program needn't handle non-finite values.
Results may differ from a plain program's by a relative error of at most 0.012.
Values may be sent and summed in bfloat16 or wider, within the bound.
A program may use at most 128 MiB of HBM per device.

v0:
```python
import jax
import jax.numpy as jnp
from jax import lax
from jax.sharding import PartitionSpec as P


def on_device(tokens, cotangent, gate_weights, routes, w_gate, w_up, w_down):
    tok_dev, width = tokens.shape
    top_k = routes.shape[1]
    groups = lax.axis_size("ep")
    narrow = lax.axis_size("tp")
    pair_count = tok_dev * top_k
    capacity = 3 * top_k * tok_dev // (2 * groups)
    quarter = width // narrow
    routed = routes.reshape(pair_count)
    onehot = (routed[:, None] == jnp.arange(groups, dtype=jnp.int32)[None, :]).astype(jnp.int32)
    earlier = jnp.sum((jnp.cumsum(onehot, axis=0) - onehot) * onehot, axis=1)
    slot_of = routed * capacity + earlier
    slot_pair = jnp.full((groups * capacity,), pair_count, jnp.int32)
    slot_pair = slot_pair.at[slot_of].set(jnp.arange(pair_count, dtype=jnp.int32))
    source_row = jnp.where(slot_pair < pair_count, slot_pair // top_k, tok_dev)
    offset = lax.axis_index("tp") * quarter
    tok_part = lax.dynamic_slice_in_dim(tokens, offset, quarter, 1)
    cot_part = lax.dynamic_slice_in_dim(cotangent, offset, quarter, 1)
    columns = tok_part.shape[1]
    zero_row = jnp.zeros((1, columns), jnp.bfloat16)
    sent_tok = jnp.concatenate([tok_part, zero_row], axis=0)[source_row].reshape(
        groups, capacity, columns
    )
    sent_cot = jnp.concatenate([cot_part, zero_row], axis=0)[source_row].reshape(
        groups, capacity, columns
    )
    gate_pad = jnp.concatenate(
        [gate_weights.reshape(pair_count), jnp.zeros((1,), jnp.bfloat16)], axis=0
    )
    sent_gate = gate_pad[slot_pair].reshape(groups, capacity)
    got_tok, got_cot, got_gate = (
        lax.all_to_all(sent_tok, "ep", split_axis=0, concat_axis=0, tiled=True),
        lax.all_to_all(sent_cot, "ep", split_axis=0, concat_axis=0, tiled=True),
        lax.all_to_all(sent_gate, "ep", split_axis=0, concat_axis=0, tiled=True),
    )
    row_total = groups * capacity
    x_rows = got_tok.reshape(row_total, columns)
    c_rows = got_cot.reshape(row_total, columns)
    x_rows, c_rows = (
        lax.all_gather(x_rows, "tp", axis=1, tiled=True),
        lax.all_gather(c_rows, "tp", axis=1, tiled=True),
    )
    weights = got_gate.reshape(row_total).astype(jnp.float32)
    weight_gate = w_gate[0]
    weight_up = w_up[0]
    weight_down = w_down[0]
    contract_last = (((1,), (1,)), ((), ()))
    contract_first = (((0,), (0,)), ((), ()))
    gate_pre = jnp.dot(x_rows, weight_gate, preferred_element_type=jnp.float32)
    up_pre = jnp.dot(x_rows, weight_up, preferred_element_type=jnp.float32)
    logistic = jax.nn.sigmoid(gate_pre)
    activated = gate_pre * logistic
    hidden = (activated * up_pre).astype(jnp.bfloat16)
    back_hidden = lax.dot_general(
        c_rows, weight_down, contract_last, preferred_element_type=jnp.float32
    )
    gate_part = jnp.sum(hidden.astype(jnp.float32) * back_hidden, axis=1)
    scaled = (weights[:, None] * c_rows.astype(jnp.float32)).astype(jnp.bfloat16)
    grad_down = lax.dot_general(
        hidden, scaled, contract_first, preferred_element_type=jnp.float32
    ).astype(jnp.bfloat16)
    grad_hidden = weights[:, None] * back_hidden
    gate_grad = (grad_hidden * up_pre * logistic * (1.0 + gate_pre * (1.0 - logistic))).astype(
        jnp.bfloat16
    )
    up_grad = (grad_hidden * activated).astype(jnp.bfloat16)
    grad_gate_w = lax.dot_general(
        x_rows, gate_grad, contract_first, preferred_element_type=jnp.float32
    ).astype(jnp.bfloat16)
    grad_up_w = lax.dot_general(
        x_rows, up_grad, contract_first, preferred_element_type=jnp.float32
    ).astype(jnp.bfloat16)
    row_part = lax.dot_general(
        gate_grad, weight_gate, contract_last, preferred_element_type=jnp.float32
    )
    row_part = row_part + lax.dot_general(
        up_grad, weight_up, contract_last, preferred_element_type=jnp.float32
    )
    combined = lax.psum_scatter(
        row_part.astype(jnp.bfloat16), "tp", scatter_dimension=1, tiled=True
    )
    gate_total = lax.psum(gate_part, "tp")
    back_rows = lax.all_to_all(
        combined.reshape(groups, capacity, quarter), "ep", split_axis=0, concat_axis=0, tiled=True
    )
    back_gate = lax.all_to_all(
        gate_total.reshape(groups, capacity), "ep", split_axis=0, concat_axis=0, tiled=True
    )
    pair_rows = back_rows.reshape(row_total, quarter)[slot_of]
    grad_tokens = jnp.sum(
        pair_rows.reshape(tok_dev, top_k, quarter).astype(jnp.float32), axis=1
    ).astype(jnp.bfloat16)
    grad_gates = back_gate.reshape(row_total)[slot_of].reshape(tok_dev, top_k)
    return (grad_tokens, grad_gates, grad_gate_w[None], grad_up_w[None], grad_down[None])


def solution(mesh):
    in_specs = (
        P("ep", None),
        P("ep", None),
        P("ep", None),
        P("ep", None),
        P("ep", None, "tp"),
        P("ep", None, "tp"),
        P("ep", "tp", None),
    )
    out_specs = (
        P("ep", "tp"),
        P("ep", None),
        P("ep", None, "tp"),
        P("ep", None, "tp"),
        P("ep", "tp", None),
    )
    return jax.shard_map(
        on_device, mesh=mesh, in_specs=in_specs, out_specs=out_specs, check_vma=False
    )
```

profile of v0, /device:TPU:0, one launch (start us, length us, event | category | flops | bytes accessed | tf_op | source)
XLA Modules:
  0.0 196.0 jit_solution(8647376752042619612)
XLA Ops:
  7.2 0.8 copy.19
  8.3 0.7 broadcast_multiply_fusion
  9.0 1.1 reduce-window.6
  10.1 0.2 slice_reduce_fusion
  10.8 2.4 %scatter_custom_fusion = s32[768]{0:T(1024)S(1)} fusion(s32[512]{0:T(512)S(1)} %bitcast.55, s32[512]{0:T(512)S(1)} %iota.11, s32[]{:T(128)} %constant.16.clone.1), kind=kCustom, calls=%fused_computation.51 | custom fusion | bytes 3076 | tf_op jit(solution)/shard_map/scatter | solution.py:20
  13.3 1.1 constant_dynamic-slice_fusion
  14.4 2.7 %gather_fusion.2 = bf16[768,512]{1,0:T(8,128)(2,1)S(1)} fusion(bf16[257,512]{1,0:T(8,128)(2,1)S(1)} %concatenate.11, s32[1024]{0:T(1024)S(1)} %get-tuple-element.23), kind=kCustom, calls=%fused_computation.2 | custom fusion | bytes 1575936 | tf_op jit(solution)/shard_map/gather | solution.py:27
  17.1 27.4 %all_to_all.34 = bf16[8,96,512]{2,1,0:T(8,128)(2,1)} all-to-all(bf16[8,96,512]{2,1,0:T(8,128)(2,1)S(1)} %bitcast.51), channel_id=1, replica_groups=mesh['ep'=8,'tp'=4] {'ep'}, dimensions={0} | all-to-all | bytes 1572864 | tf_op jit(solution)/shard_map/all_to_all | solution.py:38
  44.6 2.7 %gather_fusion.1 = bf16[768,512]{1,0:T(8,128)(2,1)S(1)} fusion(bf16[257,512]{1,0:T(8,128)(2,1)S(1)} %concatenate.10, s32[1024]{0:T(1024)S(1)} %get-tuple-element.23), kind=kCustom, calls=%fused_computation.1 | custom fusion | bytes 1575936 | tf_op jit(solution)/shard_map/gather | solution.py:30
  47.3 23.3 %all_to_all.35 = bf16[8,96,512]{2,1,0:T(8,128)(2,1)} all-to-all(bf16[8,96,512]{2,1,0:T(8,128)(2,1)S(1)} %bitcast.50), channel_id=1, replica_groups=mesh['ep'=8,'tp'=4] {'ep'}, dimensions={0} | all-to-all | bytes 1572864 | tf_op jit(solution)/shard_map/all_to_all | solution.py:39
  70.9 5.0 %gather_fusion = bf16[768]{0:T(1024)(128)(2,1)S(1)} fusion(bf16[513]{0:T(1024)(128)(2,1)S(1)} %pad_maximum_fusion, s32[1024]{0:T(1024)S(1)} %get-tuple-element.24), kind=kCustom, calls=%fused_computation | custom fusion | bytes 6144 | tf_op jit(solution)/shard_map/gather | solution.py:36
  76.0 9.9 %all_to_all.36 = bf16[8,1,96]{2,1,0:T(2,128)(2,1)S(1)} all-to-all(bf16[8,1,96]{2,1,0:T(2,128)(2,1)S(1)} %all_to_all.28), channel_id=1, replica_groups=mesh['ep'=8,'tp'=4] {'ep'}, dimensions={0} | all-to-all | bytes 3072 | tf_op jit(solution)/shard_map/all_to_all | solution.py:40
  86.0 8.1 %fusion.2 = f32[768,896]{1,0:T(8,128)} fusion(bf16[768,2048]{1,0:T(8,128)(2,1)} %all-gather.5.cloned.1.call-done, bf16[1,2048,896]{2,1,0:T(8,128)(2,1)} %param.11), kind=kOutput, calls=%fused_computation.10 | convolution fusion | flops 2818572288 | bytes 9568256 | tf_op jit(solution)/shard_map/dot_general | solution.py:55
  94.1 4.9 %fusion.6 = f32[768,896]{1,0:T(8,128)} fusion(bf16[768,2048]{1,0:T(8,128)(2,1)S(1)} %copy-done.4, bf16[1,2048,896]{2,1,0:T(8,128)(2,1)S(1)} %copy-done.2), kind=kOutput, calls=%fused_computation.14 | convolution fusion | flops 2818572288 | bytes 9568256 | tf_op jit(solution)/shard_map/dot_general | solution.py:56
  99.1 3.2 %all-gather.3.cloned.1.call-done = bf16[768,2048]{1,0:T(8,128)(2,1)} async-done(((bf16[768,512]{1,0:T(8,128)(2,1)}), bf16[768,2048]{1,0:T(8,128)(2,1)}) %all-gather.3.cloned.1.call-update) | async-done | bytes 3145744 | tf_op jit(solution)/shard_map/all_gather | solution.py:47
  102.2 9.9 %multiply_reduce_fusion = (f32[768]{0:T(1024)S(1)}, bf16[768,896]{1,0:T(8,128)(2,1)}, bf16[768,896]{1,0:T(8,128)(2,1)S(1)}, bf16[768,896]{1,0:T(8,128)(2,1)S(1)}) fusion(f32[768,896]{1,0:T(8,128)} %fusion.6, f32[768,896]{1,0:T(8,128)} %fusion.2, f32[768]{0:T(1024)S(1)} %reshape.115, bf16[768,2048]{1,0:T(8,128)(2,1)} %all-gather.3.cloned.1.call-done, ...), kind=kOutput, calls=%fused_computation.22 | convolution fusion | flops 2831645952 | bytes 16455680 | tf_op jit(solution)/shard_map/dot_general | solution.py:60
  112.1 3.4 %fusion = f32[768,2048]{1,0:T(8,128)S(1)} fusion(bf16[768,896]{1,0:T(8,128)(2,1)S(1)} %get-tuple-element.17, bf16[1,2048,896]{2,1,0:T(8,128)(2,1)S(1)} %copy-done.1), kind=kOutput, calls=%fused_computation.8 | convolution fusion | flops 2818572288 | bytes 11337728 | tf_op jit(solution)/shard_map/dot_general | solution.py:79
  115.6 4.9 %add_convert_fusion = bf16[768,2048]{1,0:T(8,128)(2,1)} fusion(f32[768,2048]{1,0:T(8,128)S(1)} %fusion, bf16[768,896]{1,0:T(8,128)(2,1)S(1)} %get-tuple-element.18, bf16[1,2048,896]{2,1,0:T(8,128)(2,1)S(1)} %copy-done.3), kind=kOutput, calls=%fused_computation.7 | convolution fusion | flops 2821718016 | bytes 14483456 | tf_op jit(solution)/shard_map/dot_general | solution.py:82
  120.5 6.5 %psum.7 = f32[8,1,96]{2,1,0:T(1,128)} all-reduce(f32[8,1,96]{2,1,0:T(1,128)S(1)} %all_to_all.26), channel_id=1, replica_groups=mesh['ep'=8,'tp'=4] {'tp'}, use_global_device_ids=true, to_apply=%region_7.8 | all-reduce | flops 768 | bytes 6144 | tf_op jit(solution)/shard_map/psum | solution.py:88
  127.0 5.7 %all-to-all-start.4 = ((f32[8,1,96]{2,1,0:T(1,128)}), f32[8,1,96]{2,1,0:T(1,128)S(1)}, u32[]{:S(2)}, u32[]{:S(2)}) async-start(f32[8,1,96]{2,1,0:T(1,128)} %psum.7), calls=%async_computation.5 | async-start | bytes 8192 | tf_op jit(solution)/shard_map/all_to_all | solution.py:92
  132.7 6.4 %all-to-all-done.4 = f32[8,1,96]{2,1,0:T(1,128)S(1)} async-done(((f32[8,1,96]{2,1,0:T(1,128)}), f32[8,1,96]{2,1,0:T(1,128)S(1)}, u32[]{:S(2)}, u32[]{:S(2)}) %all-to-all-start.4) | async-done | bytes 3104 | tf_op jit(solution)/shard_map/all_to_all | solution.py:92
  139.1 19.2 %reduce-scatter.2.cloned.1.call-done = bf16[768,512]{1,0:T(8,128)(2,1)} async-done(((bf16[768,2048]{1,0:T(8,128)(2,1)}), bf16[768,512]{1,0:T(8,128)(2,1)}) %reduce-scatter.2.cloned.1.call-update) | async-done | bytes 786448 | tf_op jit(solution)/shard_map/reduce_scatter | solution.py:85
  158.3 5.5 %all-to-all-start.3 = ((bf16[8,96,512]{2,1,0:T(8,128)(2,1)}), bf16[8,96,512]{2,1,0:T(8,128)(2,1)S(1)}, u32[]{:S(2)}, u32[]{:S(2)}) async-start(bf16[8,96,512]{2,1,0:T(8,128)(2,1)} %bitcast.54), calls=%async_computation.4 | async-start | bytes 1572864 | tf_op jit(solution)/shard_map/all_to_all | solution.py:89
  163.9 7.4 %convert_bitcast_fusion.1 = bf16[1,2048,896]{2,1,0:T(8,128)(2,1)} fusion(bf16[768,2048]{1,0:T(8,128)(2,1)} %all-gather.5.cloned.1.call-done, bf16[768,896]{1,0:T(8,128)(2,1)S(1)} %get-tuple-element.18), kind=kOutput, calls=%fused_computation.19 | convolution fusion | flops 2820407296 | bytes 8192000 | tf_op jit(solution)/shard_map/dot_general | solution.py:76
  171.2 4.9 %convert_bitcast_fusion.2 = bf16[1,2048,896]{2,1,0:T(8,128)(2,1)} fusion(bf16[768,2048]{1,0:T(8,128)(2,1)S(1)} %copy-done.5, bf16[768,896]{1,0:T(8,128)(2,1)S(1)} %get-tuple-element.17), kind=kOutput, calls=%fused_computation.20 | convolution fusion | flops 2820407296 | bytes 8192000 | tf_op jit(solution)/shard_map/dot_general | solution.py:73
  176.2 4.7 %convert_bitcast_fusion = bf16[1,896,2048]{2,1,0:T(8,128)(2,1)} fusion(bf16[768,896]{1,0:T(8,128)(2,1)S(1)} %copy-done.7, bf16[768,2048]{1,0:T(8,128)(2,1)S(1)} %copy-done.6, f32[768]{0:T(1024)S(1)} %reshape.115), kind=kOutput, calls=%fused_computation.18 | convolution fusion | flops 2825125888 | bytes 8195072 | tf_op jit(solution)/shard_map/dot_general | solution.py:65
  180.8 0.5 broadcast.111
  181.3 0.7 reduce.10
  182.1 2.3 %gather_fusion.4 = f32[512]{0:T(512)S(1)} fusion(f32[768]{0:T(1024)S(1)} %reshape.113, s32[1024]{0:T(1024)S(1)} %pad_clamp_fusion), kind=kCustom, calls=%fused_computation.4 | custom fusion | bytes 6144 | tf_op jit(solution)/shard_map/gather | solution.py:99
  184.5 0.7 copy.22
  185.2 2.0 %gather_fusion.3 = bf16[512,512]{1,0:T(8,128)(2,1)S(1)} fusion(bf16[768,512]{1,0:T(8,128)(2,1)S(1)} %bitcast.49, s32[1024]{0:T(1024)S(1)} %pad_clamp_fusion), kind=kCustom, calls=%fused_computation.3 | custom fusion | bytes 1050624 | tf_op jit(solution)/shard_map/gather | solution.py:95
  187.3 2.1 %reduce_sum.34 = bf16[256,512]{1,0:T(8,128)(2,1)} reduce(bf16[256,2,512]{2,1,0:T(2,128)(2,1)S(1)} %reshape.112, bf16[]{:T(256)} %constant.42.clone.1), dimensions={1}, to_apply=%region_5.6 | reduce | flops 131072 | bytes 786434 | tf_op jit(solution)/shard_map/reduce_sum | solution.py:96
  (49 shorter events, 2.0 us)
Async XLA Ops:
  7.2 78.8 %all-gather.5.cloned.1.call-start = ((), (), s32[]{:S(2)}) async-start(), calls=%async_computation.7 | async-start | bytes 3932160 | tf_op jit(solution)/shard_map/all_gather | solution.py:46
  44.5 57.8 %all-gather.3.cloned.1.call-start = ((), (), s32[]{:S(2)}) async-start(), calls=%async_computation.6 | async-start | bytes 3932160 | tf_op jit(solution)/shard_map/all_gather | solution.py:47
  44.6 26.1 %copy-start = (bf16[256,2]{0,1:T(2,128)(2,1)S(1)}, bf16[256,2]{0,1:T(2,128)(2,1)}, u32[]{:S(2)}) copy-start(bf16[256,2]{0,1:T(2,128)(2,1)} %param.9) | copy-start | bytes 3076
  70.6 87.8 %reduce-scatter.2.cloned.1.call-start = ((), (), s32[]{:S(2)}) async-start(), calls=%async_computation.8 | async-start | bytes 3932160 | tf_op jit(solution)/shard_map/reduce_scatter | solution.py:85
  86.0 8.1 %copy-start.2 = (bf16[1,2048,896]{2,1,0:T(8,128)(2,1)S(1)}, bf16[1,2048,896]{2,1,0:T(8,128)(2,1)}, u32[]{:S(2)}) copy-start(bf16[1,2048,896]{2,1,0:T(8,128)(2,1)} %param.12) | copy-start | bytes 11010052
  86.0 8.1 %copy-start.4 = (bf16[768,2048]{1,0:T(8,128)(2,1)S(1)}, bf16[768,2048]{1,0:T(8,128)(2,1)}, u32[]{:S(2)}) copy-start(bf16[768,2048]{1,0:T(8,128)(2,1)} %all-gather.5.cloned.1.call-done) | copy-start | bytes 9437188
  102.2 9.9 %copy-start.1 = (bf16[1,2048,896]{2,1,0:T(8,128)(2,1)S(1)}, bf16[1,2048,896]{2,1,0:T(8,128)(2,1)}, u32[]{:S(2)}) copy-start(bf16[1,2048,896]{2,1,0:T(8,128)(2,1)} %param.11) | copy-start | bytes 11010052
  112.1 3.5 %copy-start.3 = (bf16[1,2048,896]{2,1,0:T(8,128)(2,1)S(1)}, bf16[1,2048,896]{2,1,0:T(8,128)(2,1)}, u32[]{:S(2)}) copy-start(bf16[1,2048,896]{2,1,0:T(8,128)(2,1)} %param.12) | copy-start | bytes 11010052
  127.0 12.1 %all-to-all-start.4 = ((f32[8,1,96]{2,1,0:T(1,128)}), f32[8,1,96]{2,1,0:T(1,128)S(1)}, u32[]{:S(2)}, u32[]{:S(2)}) async-start(f32[8,1,96]{2,1,0:T(1,128)} %psum.7), calls=%async_computation.5 | async-start | bytes 8192 | tf_op jit(solution)/shard_map/all_to_all | solution.py:92
  158.3 26.8 %all-to-all-start.3 = ((bf16[8,96,512]{2,1,0:T(8,128)(2,1)}), bf16[8,96,512]{2,1,0:T(8,128)(2,1)S(1)}, u32[]{:S(2)}, u32[]{:S(2)}) async-start(bf16[8,96,512]{2,1,0:T(8,128)(2,1)} %bitcast.54), calls=%async_computation.4 | async-start | bytes 1572864 | tf_op jit(solution)/shard_map/all_to_all | solution.py:89
  163.9 7.4 %copy-start.5 = (bf16[768,2048]{1,0:T(8,128)(2,1)S(1)}, bf16[768,2048]{1,0:T(8,128)(2,1)}, u32[]{:S(2)}) copy-start(bf16[768,2048]{1,0:T(8,128)(2,1)} %all-gather.5.cloned.1.call-done) | copy-start | bytes 9437188
  171.2 4.9 %copy-start.6 = (bf16[768,2048]{1,0:T(8,128)(2,1)S(1)}, bf16[768,2048]{1,0:T(8,128)(2,1)}, u32[]{:S(2)}) copy-start(bf16[768,2048]{1,0:T(8,128)(2,1)} %all-gather.3.cloned.1.call-done) | copy-start | bytes 9437188
  171.2 4.9 %copy-start.7 = (bf16[768,896]{1,0:T(8,128)(2,1)S(1)}, bf16[768,896]{1,0:T(8,128)(2,1)}, u32[]{:S(2)}) copy-start(bf16[768,896]{1,0:T(8,128)(2,1)} %get-tuple-element.16) | copy-start | bytes 4128772
Sparse Core Ops, SparseCore 0:
  44.6 27.5 all-gather.4
  73.8 28.4 all-gather.2
  120.6 37.7 reduce-scatter.1
where the time goes:
time: 196 us
  blocking collectives  67 us (34%)
  matrix products  48.2 us (25%)
  waiting for transfers between devices  28.9 us (15%)
  local copies, waits for them, and re-layouts  21.9 us (11%)
  between operations  14 us (7%)
  starting transfers between devices  11.3 us (6%)
  other arithmetic  4.75 us (2%)
    all_to_all x1, blocking collectives, on_device(): lax.all_to_all(sent_tok, 'ep', split_axis=0, concat_axis=0, tiled=True)  27.4 us
    all_to_all x1, blocking collectives, on_device(): lax.all_to_all(sent_cot, 'ep', split_axis=0, concat_axis=0, tiled=True)  23.3 us
    reduce_scatter x1, waiting for transfers between devices, on_device(): lax.psum_scatter(row_part.astype(jnp.bfloat16), 'tp', scatter_dimension=1...  19.2 us
    dot_general x1, matrix products, on_device(): lax.dot_general(c_rows, weight_down, contract_last, preferred_element_typ...  9.87 us
    all_to_all x1, blocking collectives, on_device(): lax.all_to_all(sent_gate, 'ep', split_axis=0, concat_axis=0, tiled=True)  9.87 us
    dot_general x1, matrix products, on_device(): gate_pre = jnp.dot(x_rows, weight_gate, preferred_element_type=jnp.float32)  8.1 us
    dot_general x1, matrix products, on_device(): lax.dot_general(x_rows, up_grad, contract_first, preferred_element_type=j...  7.35 us
    psum x1, blocking collectives, on_device(): gate_total = lax.psum(gate_part, 'tp')  6.47 us
  transfers between devices with their start and end apart: 5, of which 3 were waited for; matrix products, arithmetic and copies ran while one was open for 22% of the time, Pallas kernels for 0%

commit v1 on v0

v1 whole, which is shorter than its diff:
```python
import functools

import jax
import jax.numpy as jnp
from jax import lax
from jax.experimental import pallas as pl
from jax.experimental.pallas import tpu as pltpu
from jax.sharding import PartitionSpec as P

MESH = pl.DeviceIdType.MESH
LAST = (((1,), (1,)), ((), ()))
FIRST = (((0,), (0,)), ((), ()))
GATE_ROWS = 16
SUM_ROWS = 8


def expert_kernel(groups, slot, quarter,
                  sent_tok, sent_cot, sent_gate, w_gate, w_up, w_down,
                  back_rows, back_gate, out_gate, out_up, out_down,
                  x_rows, c_rows, gates, wg, wu, wd, gate_pre, up_pre, back, hidden, grads,
                  part, core_got, x_got, total, gate_all, gate_sum,
                  og, ou, od,
                  load_sem, near_sem, first_send, first_recv, core_send, core_recv,
                  x_send, x_recv, second_send, second_recv, gate_send, gate_recv,
                  pair_send, pair_recv, cross_send, cross_recv, home_send, home_recv,
                  sum_send, sum_recv, sumhome_send, sumhome_recv, out_sem):
    me = lax.axis_index("ep")
    t = lax.axis_index("tp")
    core = lax.rem(t, 2)
    side = t // 2
    core_peer = side * 2 + (1 - core)
    x_peer = (1 - side) * 2 + core
    rows = groups * slot
    ffe = wg.shape[1]
    width = wg.shape[0]

    barrier = pltpu.get_barrier_semaphore()

    def greet(d, _):
        pl.semaphore_signal(barrier, inc=1, device_id=(lax.rem(me + d, groups), t),
                            device_id_type=MESH)
        return 0

    loads = [
        pltpu.make_async_copy(w_gate, wg, load_sem.at[0]),
        pltpu.make_async_copy(w_up, wu, load_sem.at[1]),
        pltpu.make_async_copy(w_down, wd, load_sem.at[2]),
    ]
    lax.fori_loop(1, groups, greet, 0)
    for o in range(1, 4):
        pl.semaphore_signal(barrier, inc=1, device_id=(me, lax.rem(t + o, 4)),
                            device_id_type=MESH)
    for load in loads:
        load.start()
    pl.semaphore_wait(barrier, groups + 2)

    def rblk(ref, s, size=slot):
        return ref.at[pl.ds(pl.multiple_of(s * size, size if size < 16 else 16), size)]

    def blk(ref, s, q):
        return ref.at[pl.ds(pl.multiple_of(s * slot, 16), slot),
                      pl.ds(pl.multiple_of(q * quarter, 128), quarter)]

    def rc(src, dst, ssem, rsem, ep, tp):
        return pltpu.make_async_remote_copy(
            src_ref=src, dst_ref=dst, send_sem=ssem, recv_sem=rsem,
            device_id=(ep, tp), device_id_type=MESH)

    def loop(lo, hi, body):
        def step(d, c):
            body(d)
            return c
        lax.fori_loop(lo, hi, step, 0)

    sent = (sent_tok, sent_cot)
    full = (x_rows, c_rows)

    def first(a, d, land):
        to = lax.rem(me + d, groups)
        return rc(rblk(sent[a], to), blk(full[a], land, t), first_send.at[a, d],
                  first_recv.at[a, d], to, t)

    def gate_copy(d, land):
        to = lax.rem(me + d, groups)
        return rc(rblk(sent_gate, to, GATE_ROWS), rblk(gates, land, GATE_ROWS),
                  gate_send.at[d], gate_recv.at[d], to, t)

    def source(d):
        return lax.rem(me - d + groups, groups)

    def to_core(a, d, q):
        s = source(d)
        return rc(blk(full[a], s, q), blk(full[a], s, q), core_send.at[a, d],
                  core_recv.at[a, d], me, core_peer)

    def to_x(a, d, q):
        s = source(d)
        return rc(blk(full[a], s, q), blk(full[a], s, q), x_send.at[a, d],
                  x_recv.at[a, d], me, x_peer)

    def to_core_again(a, d, q):
        s = source(d)
        return rc(blk(full[a], s, q), blk(full[a], s, q), second_send.at[a, d],
                  second_recv.at[a, d], me, core_peer)

    x_core_peer = (1 - side) * 2 + (1 - core)

    for a in range(2):
        loop(1, groups, lambda d, a=a: first(a, d, me).start())
        if a == 0:
            loop(1, groups, lambda d: gate_copy(d, me).start())
    near = [pltpu.make_async_copy(rblk(sent[a], me), blk(full[a], me, t), near_sem.at[a])
            for a in range(2)]
    near.append(pltpu.make_async_copy(rblk(sent_gate, me, GATE_ROWS), rblk(gates, me, GATE_ROWS),
                                      near_sem.at[2]))
    for copy in near:
        copy.start()
    for copy in near:
        copy.wait()

    def forward(a, d):
        to_x(a, d, t).start()
        to_core(a, d, t).start()

    def stage1(a, d):
        first(a, d, source(d)).wait_recv()
        forward(a, d)

    def stage2(a, d):
        to_x(a, d, x_peer).wait_recv()
        to_core_again(a, d, x_peer).start()

    def settle(a):
        def body(d):
            to_core(a, d, core_peer).wait_recv()
            to_core_again(a, d, x_core_peer).wait_recv()
        loop(0, groups, body)

    def both(a):
        def body(d):
            stage1(a, d)
            stage2(a, d - 1)
        return body

    forward(0, 0)
    loop(1, groups, both(0))
    stage2(0, groups - 1)
    forward(1, 0)
    settle(0)
    loads[0].wait()
    loads[1].wait()

    half = rows // 2
    chunks = []
    at = 0
    while at < ffe:
        chunks.append((at, min(256, ffe - at)))
        at += 256
    pieces = [(w, o, lo, n) for lo, n in chunks for w, o in ((wg, gate_pre), (wu, up_pre))]

    def product(lhs, w, o, lo, n):
        def body(h):
            r = pl.ds(pl.multiple_of(h * half, 16), half)
            o[r, lo:lo + n] = jnp.dot(lhs[r, :], w[:, lo:lo + n],
                                      preferred_element_type=jnp.float32)
        loop(0, 2, body)

    count = len(pieces)
    for i, (w, o, lo, n) in enumerate(pieces):
        product(x_rows, w, o, lo, n)
        lower, upper = max(1, i * groups // count), (i + 1) * groups // count
        if upper > lower:
            loop(lower, upper, both(1))
    stage2(1, groups - 1)
    settle(1)
    loop(1, groups, lambda d: gate_copy(d, source(d)).wait_recv())
    loads[2].wait()

    def back_product(lo, n):
        def body(h):
            r = pl.ds(pl.multiple_of(h * half, 16), half)
            back[r, lo:lo + n] = lax.dot_general(
                c_rows[r, :], wd[lo:lo + n, :], LAST, preferred_element_type=jnp.float32)
        loop(0, 2, body)

    for lo, n in chunks:
        back_product(lo, n)

    lanes = gates.shape[1]
    eye = (lax.broadcasted_iota(jnp.int32, (slot, lanes), 0)
           == lax.broadcasted_iota(jnp.int32, (slot, lanes), 1)).astype(jnp.bfloat16)

    def weight_of(s):
        g = gates[pl.ds(pl.multiple_of(s * GATE_ROWS, GATE_ROWS), GATE_ROWS), :]
        return lax.dot_general(eye, g, LAST, preferred_element_type=jnp.float32)[:, 0:1]

    def elementwise(s):
        r = pl.ds(pl.multiple_of(s * slot, 16), slot)
        weight = weight_of(s)
        summed = jnp.zeros((slot, 128), jnp.float32)
        for lo in range(0, ffe, 128):
            g = gate_pre[r, lo:lo + 128]
            u = up_pre[r, lo:lo + 128]
            b = back[r, lo:lo + 128]
            logistic = jax.nn.sigmoid(g)
            act = g * logistic
            h = (act * u).astype(jnp.bfloat16)
            hidden[r, lo:lo + 128] = h
            summed = summed + h.astype(jnp.float32) * b
            gh = weight * b
            grads[r, lo:lo + 128] = (gh * u * logistic * (1.0 + g * (1.0 - logistic))).astype(
                jnp.bfloat16)
            grads[r, ffe + lo:ffe + lo + 128] = (gh * act).astype(jnp.bfloat16)
        padded = jnp.concatenate(
            [summed, jnp.zeros((lanes - slot, 128), jnp.float32)], axis=0) if lanes > slot else summed
        row = jnp.sum(padded.T, axis=0, keepdims=True)
        gate_all[t, pl.ds(pl.multiple_of(s * SUM_ROWS, SUM_ROWS), SUM_ROWS), :] = jnp.broadcast_to(
            row, (SUM_ROWS, lanes))
        cs = c_rows[r, :].astype(jnp.float32) * weight
        c_rows[r, :] = cs.astype(jnp.bfloat16)

    def drain(a):
        def body(d):
            to_core(a, d, t).wait_send()
            to_x(a, d, t).wait_send()
            to_core_again(a, d, x_peer).wait_send()
        loop(0, groups, body)
        loop(1, groups, lambda d: first(a, d, me).wait_send())

    drain(1)
    loop(0, groups, elementwise)

    sums = [rc(gate_all.at[t], gate_all.at[t], sum_send.at[o - 1], sum_recv.at[o - 1],
               me, lax.rem(t + o, 4)) for o in range(1, 4)]
    for copy in sums:
        copy.start()

    def row_product(q, store):
        cols = pl.ds(pl.multiple_of(q * quarter, 128), quarter)

        def body(h):
            r = pl.ds(pl.multiple_of(h * half, 16), half)
            value = lax.dot_general(grads[r, 0:ffe], wg[cols, :], LAST,
                                    preferred_element_type=jnp.float32)
            value = value + lax.dot_general(grads[r, ffe:2 * ffe], wu[cols, :], LAST,
                                            preferred_element_type=jnp.float32)
            store(r, value.astype(jnp.bfloat16))
        loop(0, 2, body)

    def store_part(i):
        def store(r, value):
            part[i, r, :] = value
        return store

    pairs = [rc(part.at[i], core_got.at[i], pair_send.at[i], pair_recv.at[i], me, core_peer)
             for i in range(2)]
    row_product((1 - side) * 2 + (1 - core), store_part(0))
    pairs[0].start()
    row_product(x_peer, store_part(2))
    pairs[0].wait_recv()

    def cross(s):
        return rc(rblk(part.at[2], s), rblk(x_got, s), cross_send.at[s], cross_recv.at[s],
                  me, x_peer)

    def add_cross(d):
        s = lax.rem(me + d, groups)
        r = pl.ds(pl.multiple_of(s * slot, 16), slot)
        part[2, r, :] = (part[2, r, :].astype(jnp.float32)
                         + core_got[0, r, :].astype(jnp.float32)).astype(jnp.bfloat16)
        cross(s).start()

    loop(1, groups + 1, add_cross)
    row_product(side * 2 + (1 - core), store_part(1))
    pairs[1].start()
    row_product(t, store_part(3))
    for copy in sums:
        copy.wait_recv()
    gate_sum[...] = (gate_all[0] + gate_all[1]) + (gate_all[2] + gate_all[3])

    def sum_home(d, land):
        to = lax.rem(me + d, groups)
        return rc(rblk(gate_sum, to, SUM_ROWS), rblk(back_gate, land, SUM_ROWS),
                  sumhome_send.at[d], sumhome_recv.at[d], to, t)

    loop(1, groups, lambda d: sum_home(d, me).start())
    last = pltpu.make_async_copy(rblk(gate_sum, me, SUM_ROWS), rblk(back_gate, me, SUM_ROWS),
                                 near_sem.at[2])
    last.start()
    pairs[1].wait_recv()

    def home(d, land):
        to = lax.rem(me + d, groups)
        return rc(rblk(total, to), rblk(back_rows, land), home_send.at[d], home_recv.at[d], to, t)

    def finish(d):
        s = lax.rem(me + d, groups)
        r = pl.ds(pl.multiple_of(s * slot, 16), slot)
        cross(s).wait_recv()
        total[r, :] = (part[3, r, :].astype(jnp.float32) + core_got[1, r, :].astype(jnp.float32)
                       + x_got[r, :].astype(jnp.float32)).astype(jnp.bfloat16)

    def finish_send(d):
        finish(d)
        home(d, me).start()

    outs = []
    work = []

    def x_grad(lo, n, i):
        def run():
            left = x_rows[:, lo:lo + n]
            og[lo:lo + n, :] = lax.dot_general(
                left, grads[:, 0:ffe], FIRST, preferred_element_type=jnp.float32
            ).astype(jnp.bfloat16)
            ou[lo:lo + n, :] = lax.dot_general(
                left, grads[:, ffe:2 * ffe], FIRST, preferred_element_type=jnp.float32
            ).astype(jnp.bfloat16)
            for j, (src, dst) in enumerate(((og, out_gate), (ou, out_up))):
                copy = pltpu.make_async_copy(src.at[lo:lo + n], dst.at[lo:lo + n],
                                             out_sem.at[i, j])
                copy.start()
                outs.append(copy)
        return run

    def down_grad(lo, n, i):
        def run():
            od[lo:lo + n, :] = lax.dot_general(
                hidden[:, lo:lo + n], c_rows[...], FIRST, preferred_element_type=jnp.float32
            ).astype(jnp.bfloat16)
            copy = pltpu.make_async_copy(od.at[lo:lo + n], out_down.at[lo:lo + n],
                                         out_sem.at[i, 2])
            copy.start()
            outs.append(copy)
        return run

    step = 256
    for i, lo in enumerate(range(0, width, step)):
        work.append(x_grad(lo, min(step, width - lo), i))
    for i, (lo, n) in enumerate(chunks):
        work.append(down_grad(lo, n, i))
    lead = len(work) - 1
    for i, run in enumerate(work):
        run()
        lower, upper = max(1, 1 + i * (groups - 1) // lead), min(groups, 1 + (i + 1) * (groups - 1) // lead)
        if upper > lower:
            loop(lower, upper, finish_send)
    finish(0)
    own = pltpu.make_async_copy(rblk(total, me), rblk(back_rows, me), near_sem.at[0])
    own.start()

    loop(1, groups, lambda d: home(d, source(d)).wait_recv())
    loop(1, groups, lambda d: sum_home(d, source(d)).wait_recv())
    own.wait()
    last.wait()
    drain(0)
    loop(1, groups, lambda d: gate_copy(d, me).wait_send())
    for copy in sums + pairs:
        copy.wait_send()
    loop(0, groups, lambda s: cross(s).wait_send())
    loop(1, groups, lambda d: home(d, me).wait_send())
    loop(1, groups, lambda d: sum_home(d, me).wait_send())
    for copy in outs:
        copy.wait()


def on_device(tokens, cotangent, gate_weights, routes, w_gate, w_up, w_down):
    tok_dev, width = tokens.shape
    top_k = routes.shape[1]
    groups = lax.axis_size("ep")
    narrow = lax.axis_size("tp")
    pair_count = tok_dev * top_k
    capacity = 3 * top_k * tok_dev // (2 * groups)
    slot = -(-capacity // 16) * 16
    quarter = width // narrow
    ffe = w_gate.shape[2]
    rows = groups * slot
    lanes = -(-slot // 128) * 128
    routed = routes.reshape(pair_count)
    onehot = (routed[:, None] == jnp.arange(groups, dtype=jnp.int32)[None, :])
    before = (jnp.arange(pair_count, dtype=jnp.int32)[:, None]
              > jnp.arange(pair_count, dtype=jnp.int32)[None, :])
    counts = jnp.dot(before.astype(jnp.bfloat16), onehot.astype(jnp.bfloat16),
                     preferred_element_type=jnp.float32).astype(jnp.int32)
    earlier = jnp.sum(jnp.where(onehot, counts, 0), axis=1)
    slot_of = (routed * slot + earlier).reshape(tok_dev, top_k)
    places = jnp.arange(rows, dtype=jnp.int32)
    hits = [slot_of[:, k][:, None] == places[None, :] for k in range(top_k)]
    picked = hits[0]
    for hit in hits[1:]:
        picked = picked | hit
    select = picked.astype(jnp.bfloat16)
    offset = lax.axis_index("tp") * quarter
    tok_part = lax.dynamic_slice_in_dim(tokens, offset, quarter, 1)
    cot_part = lax.dynamic_slice_in_dim(cotangent, offset, quarter, 1)
    contract_first = (((0,), (0,)), ((), ()))
    sent_tok = lax.dot_general(select, tok_part, contract_first,
                               preferred_element_type=jnp.float32).astype(jnp.bfloat16)
    sent_cot = lax.dot_general(select, cot_part, contract_first,
                               preferred_element_type=jnp.float32).astype(jnp.bfloat16)
    gate_row = jnp.zeros((rows,), jnp.float32)
    for k in range(top_k):
        gate_row = gate_row + jnp.sum(
            jnp.where(hits[k], gate_weights[:, k].astype(jnp.float32)[:, None], 0.0), axis=0)
    sent_gate = jnp.pad(gate_row.reshape(groups, slot), ((0, 0), (0, lanes - slot)))
    sent_gate = jnp.broadcast_to(
        sent_gate.astype(jnp.bfloat16)[:, None, :], (groups, GATE_ROWS, lanes)
    ).reshape(groups * GATE_ROWS, lanes)
    vmem = pl.BlockSpec(memory_space=pltpu.VMEM)
    hbm = pl.BlockSpec(memory_space=pl.ANY)
    bf, f32 = jnp.bfloat16, jnp.float32
    dma = pltpu.SemaphoreType.DMA
    per = dma((groups,))
    twice = dma((2, groups))
    steps = max(-(-width // 256), -(-ffe // 256))
    back_rows, back_gate, grad_gate_w, grad_up_w, grad_down = pl.pallas_call(
        functools.partial(expert_kernel, groups, slot, quarter),
        out_shape=(
            jax.ShapeDtypeStruct((rows, quarter), bf),
            jax.ShapeDtypeStruct((groups * SUM_ROWS, lanes), f32),
            jax.ShapeDtypeStruct((width, ffe), bf),
            jax.ShapeDtypeStruct((width, ffe), bf),
            jax.ShapeDtypeStruct((ffe, width), bf),
        ),
        in_specs=[vmem, vmem, vmem, hbm, hbm, hbm],
        out_specs=(vmem, vmem, hbm, hbm, hbm),
        scratch_shapes=[
            pltpu.VMEM((rows, width), bf),
            pltpu.VMEM((rows, width), bf),
            pltpu.VMEM((groups * GATE_ROWS, lanes), bf),
            pltpu.VMEM((width, ffe), bf),
            pltpu.VMEM((width, ffe), bf),
            pltpu.VMEM((ffe, width), bf),
            pltpu.VMEM((rows, ffe), f32),
            pltpu.VMEM((rows, ffe), f32),
            pltpu.VMEM((rows, ffe), f32),
            pltpu.VMEM((rows, ffe), bf),
            pltpu.VMEM((rows, 2 * ffe), bf),
            pltpu.VMEM((4, rows, quarter), bf),
            pltpu.VMEM((2, rows, quarter), bf),
            pltpu.VMEM((rows, quarter), bf),
            pltpu.VMEM((rows, quarter), bf),
            pltpu.VMEM((4, groups * SUM_ROWS, lanes), f32),
            pltpu.VMEM((groups * SUM_ROWS, lanes), f32),
            pltpu.VMEM((width, ffe), bf),
            pltpu.VMEM((width, ffe), bf),
            pltpu.VMEM((ffe, width), bf),
            dma((3,)), dma((3,)),
            twice, twice, twice, twice, twice, twice, twice, twice,
            per, per,
            dma((2,)), dma((2,)),
            per, per, per, per,
            dma((3,)), dma((3,)),
            per, per,
            dma((steps, 3)),
        ],
        compiler_params=pltpu.CompilerParams(
            collective_id=0, has_side_effects=True, vmem_limit_bytes=67043328),
    )(sent_tok, sent_cot, sent_gate, w_gate[0], w_up[0], w_down[0])
    grad_tokens = jnp.dot(select, back_rows, preferred_element_type=f32).astype(bf)
    gate_line = back_gate.reshape(groups, SUM_ROWS, lanes)[:, 0, :slot].reshape(rows)
    grad_gates = jnp.stack(
        [jnp.sum(jnp.where(hit, gate_line[None, :], 0.0), axis=1) for hit in hits], axis=1)
    return (grad_tokens, grad_gates, grad_gate_w[None], grad_up_w[None], grad_down[None])


def solution(mesh):
    in_specs = (
        P("ep", None),
        P("ep", None),
        P("ep", None),
        P("ep", None),
        P("ep", None, "tp"),
        P("ep", None, "tp"),
        P("ep", "tp", None),
    )
    out_specs = (
        P("ep", "tp"),
        P("ep", None),
        P("ep", None, "tp"),
        P("ep", None, "tp"),
        P("ep", "tp", None),
    )
    return jax.shard_map(
        on_device, mesh=mesh, in_specs=in_specs, out_specs=out_specs, check_vma=False
    )
```

time: 196 us -> 126 us (0.64)
  Pallas kernels: 0 us -> 101 us
  blocking collectives: 67 us -> 0 us
  matrix products: 48.2 us -> 7.36 us
  waiting for transfers between devices: 28.9 us -> 0 us
  between operations: 14 us -> 0.7 us
  starting transfers between devices: 11.3 us -> 0 us
  local copies, waits for them, and re-layouts: 21.9 us -> 12.3 us
    pallas_call x0 -> x1, Pallas kernels: none -> 101 us  [on_device(): pl.pallas_call(functools.partial(expert_kernel, groups, slot, quarter), o...]
    all_to_all x3 -> x0, blocking collectives: 60.5 us -> none  [the longest x1 27.4 us: on_device(): lax.all_to_all(sent_tok, 'ep', split_axis=0, concat_axis=0, tiled=True)]
    dot_general x8 -> x4, matrix products: 48.2 us -> 7.36 us  [the longest x1 2.4 us: on_device(): lax.dot_general(select, tok_part, contract_first, preferred_element_type=...]
    reduce_scatter x1 -> x0, waiting for transfers between devices: 19.2 us -> none  [on_device(): lax.psum_scatter(row_part.astype(jnp.bfloat16), 'tp', scatter_dimension=1...]
    gather x5 -> x0, local copies, waits for them, and re-layouts: 14.6 us -> none  [the longest x1 5 us: on_device(): sent_gate = gate_pad[slot_pair].reshape(groups, capacity)]
    all_to_all x2 -> x0, starting transfers between devices: 11.2 us -> none  [the longest x1 5.67 us: on_device(): lax.all_to_all(gate_total.reshape(groups, capacity), 'ep', split_axis=0,...]
    unnamed x19 -> x12, local copies, waits for them, and re-layouts: 1.65 us -> 10.3 us
    psum x1 -> x0, blocking collectives: 6.47 us -> none  [on_device(): gate_total = lax.psum(gate_part, 'tp')]
  transfers between devices with their start and end apart: 5 -> 0, of which waited for: 3 -> 0; matrix products, arithmetic and copies ran while one was open for 22% -> 0% of each run, Pallas kernels for 0% -> 0%
where the time goes in v1:
time: 126 us; the launch traced here: 125 us
  Pallas kernels  101 us (80%)
  local copies, waits for them, and re-layouts  12.3 us (10%)
  matrix products  7.36 us (6%)
  other arithmetic  3.31 us (3%)
    pallas_call x1, Pallas kernels, on_device(): pl.pallas_call(functools.partial(expert_kernel, groups, slot, quarter), o...  101 us
    unnamed x12, local copies, waits for them, and re-layouts  10.3 us

profile of v1, /device:TPU:0, one launch (start us, length us, event | category | flops | bytes accessed | tf_op | source)
XLA Modules:
  0.0 124.9 jit_solution(9004217932677203666)
XLA Ops:
  0.6 0.8 slice_convert_fusion
  1.4 0.8 copy.21
  2.2 0.1 eq.45
  2.4 0.3 fusion.1
  2.6 0.1 reduce_sum.48
  2.8 0.1 copy.22
  2.9 0.7 multiply_add_fusion
  3.6 0.0 copy-start.2
  3.6 0.0 copy-start.3
  3.6 0.2 select_reduce_fusion.2
  3.8 0.1 add.20
  3.9 0.6 broadcast_in_dim.78
  4.5 2.4 %convolution_convert_fusion.sent_cot = bf16[768,512]{1,0:T(8,128)(2,1)} fusion(s32[256]{0:T(256)S(1)} %bitcast.28, s32[256]{0:T(256)S(1)} %bitcast.23, bf16[256,2048]{1,0:T(8,128)(2,1)} %param.8, s32[]{:T(128)S(6)} %select_n.23), kind=kOutput, calls=%fused_computation | convolution fusion | flops 202309632 | bytes 1050628 | tf_op jit(solution)/shard_map/dot_general | solution.py:399
  6.9 0.0 copy-done.2
  6.9 0.0 copy-done.3
  6.9 2.4 %convolution_convert_fusion.1.sent_tok = bf16[768,512]{1,0:T(8,128)(2,1)} fusion(s32[256]{0:T(256)S(1)} %bitcast.29, s32[256]{0:T(256)S(1)} %bitcast.24, bf16[256,2048]{1,0:T(8,128)(2,1)} %param.7, s32[]{:T(128)S(6)} %select_n.23), kind=kOutput, calls=%fused_computation.1 | convolution fusion | flops 202309632 | bytes 1050628 | tf_op jit(solution)/shard_map/dot_general | solution.py:397
  9.3 101.3 %shard_map.110 = (bf16[768,512]{1,0:T(8,128)(2,1)}, f32[64,128]{1,0:T(8,128)}, bf16[2048,896]{1,0:T(8,128)(2,1)}, bf16[2048,896]{1,0:T(8,128)(2,1)}, bf16[896,2048]{1,0:T(8,128)(2,1)}) custom-call(bf16[768,512]{1,0:T(8,128)(2,1)} %convolution_convert_fusion.1.sent_tok, bf16[768,512]{1,0:T(8,128)(2,1)} %convolution_convert_fusion.sent_cot, ...), custom_call_target="tpu_custom_call" | custom-call | tf_op jit(solution)/shard_map/pallas_call | solution.py:416
  110.6 2.3 %convolution_convert_fusion.2 = bf16[256,512]{1,0:T(8,128)(2,1)} fusion(bf16[768,512]{1,0:T(8,128)(2,1)} %get-tuple-element.10, s32[256]{0:T(256)} %bitcast.30, s32[256]{0:T(256)} %bitcast.25), kind=kOutput, calls=%fused_computation.2 | convolution fusion | flops 202047488 | bytes 1050624 | tf_op jit(solution)/shard_map/dot_general | solution.py:460
  112.9 0.8 slice_reduce_fusion
  113.7 0.1 broadcast_in_dim.79
  113.7 1.0 select_reduce_fusion.1
  114.8 0.6 pad_maximum_fusion
  115.4 0.0 copy-start.1
  115.4 4.3 %copy.26 = bf16[1,2048,896]{2,1,0:T(8,128)(2,1)} copy(bf16[1,2048,896]{2,1,0:T(8,128)(2,1)} %bitcast.17) | data formatting | bytes 7340032
  119.7 0.0 copy-done.1
  119.7 0.0 copy-start
  119.7 1.9 %copy.27 = bf16[1,2048,896]{2,1,0:T(8,128)(2,1)} copy(bf16[1,2048,896]{2,1,0:T(8,128)(2,1)S(1)} %bitcast.16) | data formatting | bytes 7340032
  121.6 1.5 %copy-done = bf16[896,2048]{1,0:T(8,128)(2,1)S(1)} copy-done((bf16[896,2048]{1,0:T(8,128)(2,1)S(1)}, bf16[896,2048]{1,0:T(8,128)(2,1)}, u32[]{:S(2)}) %copy-start) | copy-done | bytes 3670040
  123.0 1.8 %copy.28 = bf16[1,896,2048]{2,1,0:T(8,128)(2,1)} copy(bf16[1,896,2048]{2,1,0:T(8,128)(2,1)S(1)} %bitcast.15) | data formatting | bytes 7340032
  (3 shorter events, 0.0 us)
Async XLA Ops:
  3.6 3.4 %copy-start.2 = (s32[256,1]{0,1:T(1,128)}, s32[256,1]{0,1:T(1,128)S(1)}, u32[]{:S(2)}) copy-start(s32[256,1]{0,1:T(1,128)S(1)} %get-tuple-element.17) | copy-start | bytes 3076
  3.6 3.4 %copy-start.3 = (s32[256,1]{0,1:T(1,128)}, s32[256,1]{0,1:T(1,128)S(1)}, u32[]{:S(2)}) copy-start(s32[256,1]{0,1:T(1,128)S(1)} %get-tuple-element.18) | copy-start | bytes 3076
  115.4 4.3 %copy-start.1 = (bf16[2048,896]{1,0:T(8,128)(2,1)S(1)}, bf16[2048,896]{1,0:T(8,128)(2,1)}, u32[]{:S(2)}) copy-start(bf16[2048,896]{1,0:T(8,128)(2,1)} %get-tuple-element.13) | copy-start | bytes 11010052
  119.7 3.4 %copy-start = (bf16[896,2048]{1,0:T(8,128)(2,1)S(1)}, bf16[896,2048]{1,0:T(8,128)(2,1)}, u32[]{:S(2)}) copy-start(bf16[896,2048]{1,0:T(8,128)(2,1)} %get-tuple-element.14) | copy-start | bytes 11010052

commit v2 on v1

--- a/solution.py
+++ b/solution.py
@@ -15,9 +15,9 @@
 
 
 def expert_kernel(groups, slot, quarter,
-                  sent_tok, sent_cot, sent_gate, w_gate, w_up, w_down,
+                  tokens, cots, slots, weights, w_gate, w_up, w_down,
                   back_rows, back_gate, out_gate, out_up, out_down,
-                  x_rows, c_rows, gates, wg, wu, wd, gate_pre, up_pre, back, hidden, grads,
+                  sent_tok, sent_cot, sent_gate, x_rows, c_rows, gates, wg, wu, wd, gate_pre, up_pre, back, hidden, grads,
                   part, core_got, x_got, total, gate_all, gate_sum,
                   og, ou, od,
                   load_sem, near_sem, first_send, first_recv, core_send, core_recv,
@@ -52,8 +52,6 @@
                             device_id_type=MESH)
     for load in loads:
         load.start()
-    pl.semaphore_wait(barrier, groups + 2)
-
     def rblk(ref, s, size=slot):
         return ref.at[pl.ds(pl.multiple_of(s * size, size if size < 16 else 16), size)]
 
@@ -75,66 +73,95 @@
     sent = (sent_tok, sent_cot)
     full = (x_rows, c_rows)
 
-    def first(a, d, land):
+    def hits_of(d):
+        base = lax.rem(me + d, groups) * slot
+        ids = base + lax.broadcasted_iota(jnp.int32, (slot, slots.shape[1]), 0)
+        return [slots[k:k + 1, :] == ids for k in range(weights.shape[0])]
+
+    def any_of(hits):
+        found = hits[0]
+        for hit in hits[1:]:
+            found = found | hit
+        return found.astype(jnp.bfloat16)
+
+    def own_cols(ref):
+        return ref[:, pl.ds(pl.multiple_of(t * quarter, 128), quarter)]
+
+    def at_block(d, size=slot):
+        return pl.ds(pl.multiple_of(d * size, 16), size)
+
+    def pick(src, dst):
+        def body(d):
+            dst[at_block(d), :] = jnp.dot(
+                any_of(hits_of(d)), own_cols(src), preferred_element_type=jnp.float32
+            ).astype(jnp.bfloat16)
+        return body
+
+    def pick_gate(d, dst):
+        row = jnp.zeros((GATE_ROWS, slot), jnp.float32)
+        for k, hit in enumerate(hits_of(d)):
+            row = row + lax.dot_general(weights[k], hit.astype(jnp.bfloat16), LAST,
+                                        preferred_element_type=jnp.float32)
+        lanes = gates.shape[1]
+        if lanes > slot:
+            row = jnp.concatenate(
+                [row, jnp.zeros((GATE_ROWS, lanes - slot), jnp.float32)], axis=1)
+        dst[at_block(d, GATE_ROWS), :] = row.astype(jnp.bfloat16)
+
+    def first(a, d):
         to = lax.rem(me + d, groups)
-        return rc(rblk(sent[a], to), blk(full[a], land, t), first_send.at[a, d],
+        return rc(rblk(sent[a], d), blk(full[a], d, t), first_send.at[a, d],
                   first_recv.at[a, d], to, t)
 
-    def gate_copy(d, land):
+    def gate_copy(d):
         to = lax.rem(me + d, groups)
-        return rc(rblk(sent_gate, to, GATE_ROWS), rblk(gates, land, GATE_ROWS),
+        return rc(rblk(sent_gate, d, GATE_ROWS), rblk(gates, d, GATE_ROWS),
                   gate_send.at[d], gate_recv.at[d], to, t)
 
     def source(d):
         return lax.rem(me - d + groups, groups)
 
     def to_core(a, d, q):
-        s = source(d)
-        return rc(blk(full[a], s, q), blk(full[a], s, q), core_send.at[a, d],
+        return rc(blk(full[a], d, q), blk(full[a], d, q), core_send.at[a, d],
                   core_recv.at[a, d], me, core_peer)
 
     def to_x(a, d, q):
-        s = source(d)
-        return rc(blk(full[a], s, q), blk(full[a], s, q), x_send.at[a, d],
+        return rc(blk(full[a], d, q), blk(full[a], d, q), x_send.at[a, d],
                   x_recv.at[a, d], me, x_peer)
 
     def to_core_again(a, d, q):
-        s = source(d)
-        return rc(blk(full[a], s, q), blk(full[a], s, q), second_send.at[a, d],
+        return rc(blk(full[a], d, q), blk(full[a], d, q), second_send.at[a, d],
                   second_recv.at[a, d], me, core_peer)
 
     x_core_peer = (1 - side) * 2 + (1 - core)
 
-    for a in range(2):
-        loop(1, groups, lambda d, a=a: first(a, d, me).start())
-        if a == 0:
-            loop(1, groups, lambda d: gate_copy(d, me).start())
-    near = [pltpu.make_async_copy(rblk(sent[a], me), blk(full[a], me, t), near_sem.at[a])
-            for a in range(2)]
-    near.append(pltpu.make_async_copy(rblk(sent_gate, me, GATE_ROWS), rblk(gates, me, GATE_ROWS),
-                                      near_sem.at[2]))
-    for copy in near:
-        copy.start()
-    for copy in near:
-        copy.wait()
-
-    def forward(a, d):
+    loop(1, groups, pick(tokens, sent_tok))
+    pl.semaphore_wait(barrier, groups + 2)
+    loop(1, groups, lambda d: first(0, d).start())
+    loop(1, groups, lambda d: pick_gate(d, sent_gate))
+    loop(1, groups, pick(cots, sent_cot))
+    loop(1, groups, lambda d: gate_copy(d).start())
+    loop(1, groups, lambda d: first(1, d).start())
+    pick_gate(0, gates)
+    mine = any_of(hits_of(0))
+    for src, dst in ((tokens, x_rows), (cots, c_rows)):
+        dst[0:slot, :] = jnp.dot(mine, src[...], preferred_element_type=jnp.float32).astype(
+            jnp.bfloat16)
+
+    def stage1(a, d):
+        first(a, d).wait_recv()
         to_x(a, d, t).start()
         to_core(a, d, t).start()
-
-    def stage1(a, d):
-        first(a, d, source(d)).wait_recv()
-        forward(a, d)
 
     def stage2(a, d):
         to_x(a, d, x_peer).wait_recv()
         to_core_again(a, d, x_peer).start()
 
-    def settle(a):
+    def settle(a, lo, hi):
         def body(d):
             to_core(a, d, core_peer).wait_recv()
             to_core_again(a, d, x_core_peer).wait_recv()
-        loop(0, groups, body)
+        loop(lo, hi, body)
 
     def both(a):
         def body(d):
@@ -142,14 +169,14 @@
             stage2(a, d - 1)
         return body
 
-    forward(0, 0)
-    loop(1, groups, both(0))
+    stage1(0, 1)
+    loop(2, groups, both(0))
     stage2(0, groups - 1)
-    forward(1, 0)
-    settle(0)
+    settle(0, 1, groups)
     loads[0].wait()
     loads[1].wait()
 
+    mid = groups // 2
     half = rows // 2
     chunks = []
     at = 0
@@ -166,25 +193,20 @@
         loop(0, 2, body)
 
     count = len(pieces)
+    stage1(1, 1)
     for i, (w, o, lo, n) in enumerate(pieces):
         product(x_rows, w, o, lo, n)
-        lower, upper = max(1, i * groups // count), (i + 1) * groups // count
+        lower = 2 + i * (mid - 1) // count
+        upper = 2 + (i + 1) * (mid - 1) // count
         if upper > lower:
             loop(lower, upper, both(1))
-    stage2(1, groups - 1)
-    settle(1)
-    loop(1, groups, lambda d: gate_copy(d, source(d)).wait_recv())
+    loop(1, groups, lambda d: gate_copy(d).wait_recv())
     loads[2].wait()
 
-    def back_product(lo, n):
-        def body(h):
-            r = pl.ds(pl.multiple_of(h * half, 16), half)
-            back[r, lo:lo + n] = lax.dot_general(
-                c_rows[r, :], wd[lo:lo + n, :], LAST, preferred_element_type=jnp.float32)
-        loop(0, 2, body)
-
-    for lo, n in chunks:
-        back_product(lo, n)
+    def back_product(lo, n, h):
+        r = pl.ds(h * half, half)
+        back[r, lo:lo + n] = lax.dot_general(
+            c_rows[r, :], wd[lo:lo + n, :], LAST, preferred_element_type=jnp.float32)
 
     lanes = gates.shape[1]
     eye = (lax.broadcasted_iota(jnp.int32, (slot, lanes), 0)
@@ -219,84 +241,89 @@
         cs = c_rows[r, :].astype(jnp.float32) * weight
         c_rows[r, :] = cs.astype(jnp.bfloat16)
 
-    def drain(a):
+    def drain(a, lo, hi):
         def body(d):
             to_core(a, d, t).wait_send()
             to_x(a, d, t).wait_send()
             to_core_again(a, d, x_peer).wait_send()
-        loop(0, groups, body)
-        loop(1, groups, lambda d: first(a, d, me).wait_send())
-
-    drain(1)
-    loop(0, groups, elementwise)
-
-    sums = [rc(gate_all.at[t], gate_all.at[t], sum_send.at[o - 1], sum_recv.at[o - 1],
-               me, lax.rem(t + o, 4)) for o in range(1, 4)]
-    for copy in sums:
-        copy.start()
-
-    def row_product(q, store):
+        loop(lo, hi, body)
+
+    def row_product(q, i, h):
         cols = pl.ds(pl.multiple_of(q * quarter, 128), quarter)
-
-        def body(h):
-            r = pl.ds(pl.multiple_of(h * half, 16), half)
-            value = lax.dot_general(grads[r, 0:ffe], wg[cols, :], LAST,
-                                    preferred_element_type=jnp.float32)
-            value = value + lax.dot_general(grads[r, ffe:2 * ffe], wu[cols, :], LAST,
-                                            preferred_element_type=jnp.float32)
-            store(r, value.astype(jnp.bfloat16))
-        loop(0, 2, body)
-
-    def store_part(i):
-        def store(r, value):
-            part[i, r, :] = value
-        return store
-
-    pairs = [rc(part.at[i], core_got.at[i], pair_send.at[i], pair_recv.at[i], me, core_peer)
-             for i in range(2)]
-    row_product((1 - side) * 2 + (1 - core), store_part(0))
-    pairs[0].start()
-    row_product(x_peer, store_part(2))
-    pairs[0].wait_recv()
-
-    def cross(s):
-        return rc(rblk(part.at[2], s), rblk(x_got, s), cross_send.at[s], cross_recv.at[s],
+        r = pl.ds(h * half, half)
+        value = lax.dot_general(grads[r, 0:ffe], wg[cols, :], LAST,
+                                preferred_element_type=jnp.float32)
+        value = value + lax.dot_general(grads[r, ffe:2 * ffe], wu[cols, :], LAST,
+                                        preferred_element_type=jnp.float32)
+        part[i, r, :] = value.astype(jnp.bfloat16)
+
+    def pair(i, h):
+        r = pl.ds(h * half, half)
+        return rc(part.at[i, r], core_got.at[i, r], pair_send.at[i, h], pair_recv.at[i, h],
+                  me, core_peer)
+
+    def cross(d):
+        return rc(rblk(part.at[2], d), rblk(x_got, d), cross_send.at[d], cross_recv.at[d],
                   me, x_peer)
 
     def add_cross(d):
-        s = lax.rem(me + d, groups)
-        r = pl.ds(pl.multiple_of(s * slot, 16), slot)
+        r = at_block(d)
         part[2, r, :] = (part[2, r, :].astype(jnp.float32)
                          + core_got[0, r, :].astype(jnp.float32)).astype(jnp.bfloat16)
-        cross(s).start()
-
-    loop(1, groups + 1, add_cross)
-    row_product(side * 2 + (1 - core), store_part(1))
-    pairs[1].start()
-    row_product(t, store_part(3))
+        cross(d).start()
+
+    late = mid + 1
+    cuts = [late, late + (groups - late) // 3, late + 2 * (groups - late) // 3, groups]
+    for h in range(2):
+        lower, upper = h * mid, (h + 1) * mid
+        if h == 1:
+            stage2(1, groups - 1)
+        settle(1, max(1, lower), upper)
+        for lo, n in chunks:
+            back_product(lo, n, h)
+        if h == 0:
+            loop(cuts[0], cuts[1], both(1))
+        drain(1, max(1, lower), upper)
+        loop(lower, upper, elementwise)
+        if h == 0:
+            loop(cuts[1], cuts[2], both(1))
+        row_product(x_core_peer, 0, h)
+        pair(0, h).start()
+        row_product(x_peer, 2, h)
+        pair(0, h).wait_recv()
+        loop(lower, upper, add_cross)
+        if h == 0:
+            loop(cuts[2], cuts[3], both(1))
+        if h == 1:
+            sums = [rc(gate_all.at[t], gate_all.at[t], sum_send.at[o - 1], sum_recv.at[o - 1],
+                       me, lax.rem(t + o, 4)) for o in range(1, 4)]
+            for copy in sums:
+                copy.start()
+        row_product(core_peer, 1, h)
+        pair(1, h).start()
+        row_product(t, 3, h)
     for copy in sums:
         copy.wait_recv()
     gate_sum[...] = (gate_all[0] + gate_all[1]) + (gate_all[2] + gate_all[3])
 
     def sum_home(d, land):
-        to = lax.rem(me + d, groups)
-        return rc(rblk(gate_sum, to, SUM_ROWS), rblk(back_gate, land, SUM_ROWS),
-                  sumhome_send.at[d], sumhome_recv.at[d], to, t)
+        return rc(rblk(gate_sum, d, SUM_ROWS), rblk(back_gate, land, SUM_ROWS),
+                  sumhome_send.at[d], sumhome_recv.at[d], source(d), t)
 
     loop(1, groups, lambda d: sum_home(d, me).start())
-    last = pltpu.make_async_copy(rblk(gate_sum, me, SUM_ROWS), rblk(back_gate, me, SUM_ROWS),
+    last = pltpu.make_async_copy(rblk(gate_sum, 0, SUM_ROWS), rblk(back_gate, me, SUM_ROWS),
                                  near_sem.at[2])
     last.start()
-    pairs[1].wait_recv()
+    for h in range(2):
+        pair(1, h).wait_recv()
 
     def home(d, land):
-        to = lax.rem(me + d, groups)
-        return rc(rblk(total, to), rblk(back_rows, land), home_send.at[d], home_recv.at[d], to, t)
+        return rc(rblk(total, d), rblk(back_rows, land), home_send.at[d], home_recv.at[d],
+                  source(d), t)
 
     def finish(d):
-        s = lax.rem(me + d, groups)
-        r = pl.ds(pl.multiple_of(s * slot, 16), slot)
-        cross(s).wait_recv()
+        r = at_block(d)
+        cross(d).wait_recv()
         total[r, :] = (part[3, r, :].astype(jnp.float32) + core_got[1, r, :].astype(jnp.float32)
                        + x_got[r, :].astype(jnp.float32)).astype(jnp.bfloat16)
 
@@ -346,18 +373,23 @@
         if upper > lower:
             loop(lower, upper, finish_send)
     finish(0)
-    own = pltpu.make_async_copy(rblk(total, me), rblk(back_rows, me), near_sem.at[0])
+    own = pltpu.make_async_copy(rblk(total, 0), rblk(back_rows, me), near_sem.at[0])
     own.start()
 
-    loop(1, groups, lambda d: home(d, source(d)).wait_recv())
-    loop(1, groups, lambda d: sum_home(d, source(d)).wait_recv())
+    loop(1, groups, lambda d: home(d, lax.rem(me + d, groups)).wait_recv())
+    loop(1, groups, lambda d: sum_home(d, lax.rem(me + d, groups)).wait_recv())
     own.wait()
     last.wait()
-    drain(0)
-    loop(1, groups, lambda d: gate_copy(d, me).wait_send())
-    for copy in sums + pairs:
+    drain(0, 1, groups)
+    for a in range(2):
+        loop(1, groups, lambda d, a=a: first(a, d).wait_send())
+    loop(1, groups, lambda d: gate_copy(d).wait_send())
+    for copy in sums:
         copy.wait_send()
-    loop(0, groups, lambda s: cross(s).wait_send())
+    for i in range(2):
+        for h in range(2):
+            pair(i, h).wait_send()
+    loop(0, groups, lambda d: cross(d).wait_send())
     loop(1, groups, lambda d: home(d, me).wait_send())
     loop(1, groups, lambda d: sum_home(d, me).wait_send())
     for copy in outs:
@@ -390,22 +422,8 @@
     for hit in hits[1:]:
         picked = picked | hit
     select = picked.astype(jnp.bfloat16)
-    offset = lax.axis_index("tp") * quarter
-    tok_part = lax.dynamic_slice_in_dim(tokens, offset, quarter, 1)
-    cot_part = lax.dynamic_slice_in_dim(cotangent, offset, quarter, 1)
-    contract_first = (((0,), (0,)), ((), ()))
-    sent_tok = lax.dot_general(select, tok_part, contract_first,
-                               preferred_element_type=jnp.float32).astype(jnp.bfloat16)
-    sent_cot = lax.dot_general(select, cot_part, contract_first,
-                               preferred_element_type=jnp.float32).astype(jnp.bfloat16)
-    gate_row = jnp.zeros((rows,), jnp.float32)
-    for k in range(top_k):
-        gate_row = gate_row + jnp.sum(
-            jnp.where(hits[k], gate_weights[:, k].astype(jnp.float32)[:, None], 0.0), axis=0)
-    sent_gate = jnp.pad(gate_row.reshape(groups, slot), ((0, 0), (0, lanes - slot)))
-    sent_gate = jnp.broadcast_to(
-        sent_gate.astype(jnp.bfloat16)[:, None, :], (groups, GATE_ROWS, lanes)
-    ).reshape(groups * GATE_ROWS, lanes)
+    slots = jnp.pad(slot_of.T, ((0, 8 - top_k), (0, 0)), constant_values=-1)
+    weights = jnp.broadcast_to(gate_weights.T[:, None, :], (top_k, GATE_ROWS, tok_dev))
     vmem = pl.BlockSpec(memory_space=pltpu.VMEM)
     hbm = pl.BlockSpec(memory_space=pl.ANY)
     bf, f32 = jnp.bfloat16, jnp.float32
@@ -422,9 +440,12 @@
             jax.ShapeDtypeStruct((width, ffe), bf),
             jax.ShapeDtypeStruct((ffe, width), bf),
         ),
-        in_specs=[vmem, vmem, vmem, hbm, hbm, hbm],
+        in_specs=[vmem, vmem, vmem, vmem, hbm, hbm, hbm],
         out_specs=(vmem, vmem, hbm, hbm, hbm),
         scratch_shapes=[
+            pltpu.VMEM((rows, quarter), bf),
+            pltpu.VMEM((rows, quarter), bf),
+            pltpu.VMEM((groups * GATE_ROWS, lanes), bf),
             pltpu.VMEM((rows, width), bf),
             pltpu.VMEM((rows, width), bf),
             pltpu.VMEM((groups * GATE_ROWS, lanes), bf),
@@ -448,7 +469,7 @@
             dma((3,)), dma((3,)),
             twice, twice, twice, twice, twice, twice, twice, twice,
             per, per,
-            dma((2,)), dma((2,)),
+            dma((2, 2)), dma((2, 2)),
             per, per, per, per,
             dma((3,)), dma((3,)),
             per, per,
@@ -456,7 +477,7 @@
         ],
         compiler_params=pltpu.CompilerParams(
             collective_id=0, has_side_effects=True, vmem_limit_bytes=67043328),
-    )(sent_tok, sent_cot, sent_gate, w_gate[0], w_up[0], w_down[0])
+    )(tokens, cotangent, slots, weights, w_gate[0], w_up[0], w_down[0])
     grad_tokens = jnp.dot(select, back_rows, preferred_element_type=f32).astype(bf)
     gate_line = back_gate.reshape(groups, SUM_ROWS, lanes)[:, 0, :slot].reshape(rows)
     grad_gates = jnp.stack(

time: 126 us -> 134 us (1.063)
  Pallas kernels: 101 us -> 114 us
  matrix products: 7.36 us -> 2.56 us
  local copies, waits for them, and re-layouts: 12.3 us -> 14 us
    pallas_call x1, Pallas kernels: 101 us -> 114 us  [on_device(): pl.pallas_call(functools.partial(expert_kernel, groups, slot, quarter), o...]
    dot_general x2 -> x0, matrix products: 4.8 us -> none  [the longest x1 2.4 us: on_device(): lax.dot_general(select, tok_part, contract_first, preferred_element_type=...]
    unnamed x12 -> x8, local copies, waits for them, and re-layouts: 10.3 us -> 10.3 us
where the time goes in v2:
time: 134 us
  Pallas kernels  114 us (85%)
  local copies, waits for them, and re-layouts  14 us (10%)
  matrix products  2.56 us (2%)
  other arithmetic  2.31 us (2%)
    pallas_call x1, Pallas kernels, on_device(): pl.pallas_call(functools.partial(expert_kernel, groups, slot, quarter), o...  114 us
    unnamed x8, local copies, waits for them, and re-layouts  10.3 us

profile of v2, /device:TPU:0, one launch (start us, length us, event | category | flops | bytes accessed | tf_op | source)
XLA Modules:
  0.0 133.6 jit_solution(15302243444001761941)
XLA Ops:
  0.6 1.3 broadcast_in_dim.43.weights
  1.9 0.8 copy.14
  2.7 0.1 eq.45
  2.9 0.3 fusion.1
  3.2 0.1 reduce_sum.30
  3.3 0.1 copy.15
  3.4 0.7 multiply_add_fusion
  4.1 0.6 fusion.7
  4.6 0.6 pad.4.slots
  5.2 114.0 %shard_map.110 = (bf16[768,512]{1,0:T(8,128)(2,1)}, f32[64,128]{1,0:T(8,128)}, bf16[2048,896]{1,0:T(8,128)(2,1)}, bf16[2048,896]{1,0:T(8,128)(2,1)}, bf16[896,2048]{1,0:T(8,128)(2,1)}) custom-call(bf16[256,2048]{1,0:T(8,128)(2,1)} %tokens.1, bf16[256,2048]{1,0:T(8,128)(2,1)} %cots.1, s32[8,256]{1,0:T(8,128)} %pad.4.slots, ...), custom_call_target="tpu_custom_call" | custom-call | tf_op jit(solution)/shard_map/pallas_call | solution.py:434
  119.3 2.3 %convolution_convert_fusion = bf16[256,512]{1,0:T(8,128)(2,1)} fusion(bf16[768,512]{1,0:T(8,128)(2,1)} %get-tuple-element.10, s32[256]{0:T(256)} %bitcast.23, s32[256]{0:T(256)} %bitcast.21), kind=kOutput, calls=%fused_computation | convolution fusion | flops 202047488 | bytes 1050624 | tf_op jit(solution)/shard_map/dot_general | solution.py:481
  121.6 0.8 slice_reduce_fusion
  122.3 0.1 broadcast_in_dim.44
  122.4 1.0 select_reduce_fusion.1
  123.4 0.6 pad_maximum_fusion
  124.0 0.0 copy-start.1
  124.0 4.3 %copy.19 = bf16[1,2048,896]{2,1,0:T(8,128)(2,1)} copy(bf16[1,2048,896]{2,1,0:T(8,128)(2,1)} %bitcast.16) | data formatting | bytes 7340032
  128.4 0.0 copy-done.1
  128.4 0.0 copy-start
  128.4 1.9 %copy.20 = bf16[1,2048,896]{2,1,0:T(8,128)(2,1)} copy(bf16[1,2048,896]{2,1,0:T(8,128)(2,1)S(1)} %bitcast.15) | data formatting | bytes 7340032
  130.2 1.5 %copy-done = bf16[896,2048]{1,0:T(8,128)(2,1)S(1)} copy-done((bf16[896,2048]{1,0:T(8,128)(2,1)S(1)}, bf16[896,2048]{1,0:T(8,128)(2,1)}, u32[]{:S(2)}) %copy-start) | copy-done | bytes 3670040
  131.7 1.8 %copy.21 = bf16[1,896,2048]{2,1,0:T(8,128)(2,1)} copy(bf16[1,896,2048]{2,1,0:T(8,128)(2,1)S(1)} %bitcast.14) | data formatting | bytes 7340032
Async XLA Ops:
  124.0 4.3 %copy-start.1 = (bf16[2048,896]{1,0:T(8,128)(2,1)S(1)}, bf16[2048,896]{1,0:T(8,128)(2,1)}, u32[]{:S(2)}) copy-start(bf16[2048,896]{1,0:T(8,128)(2,1)} %get-tuple-element.13) | copy-start | bytes 11010052
  128.4 3.4 %copy-start = (bf16[896,2048]{1,0:T(8,128)(2,1)S(1)}, bf16[896,2048]{1,0:T(8,128)(2,1)}, u32[]{:S(2)}) copy-start(bf16[896,2048]{1,0:T(8,128)(2,1)} %get-tuple-element.14) | copy-start | bytes 11010052
